TPU v7x, 256 devices: a whole 4x4x8 slice. The times are simulated.
256 devices in a mesh: sp: 16 (over y, x), dp: 16 (over z, core).
Axes of the slice: x: 4, y: 4, z: 8, core: 2. Of those that a mesh axis runs over, the one named last changes fastest.
Arguments:
- tokens: bfloat16 [16, 4096, 2048], P('dp', 'sp'), may hold values from -200 to 200
- w_qdown: bfloat16 [2048, 512], P('dp'), may hold values from -0.125 to 0.125
- w_kvdown: bfloat16 [2048, 512], P('dp'), may hold values from -0.125 to 0.125
- w_rotary: bfloat16 [2048, 64], replicated, may hold values from -0.125 to 0.125
- q_gain: float32 [512], replicated, may hold values from 0.1 to 1.9
- kv_gain: float32 [512], replicated, may hold values from 0.1 to 1.9
- w_qup: bfloat16 [512, 3072], P('dp'), may hold values from -1 to 1
- w_kvup: bfloat16 [512, 4096], P('dp'), may hold values from -1 to 1
- w_out: bfloat16 [2048, 2048], P(None, 'dp'), may hold values from -0.125 to 0.125
- out_gain: float32 [2048], replicated, may hold values from 0.1 to 1.9
Outputs:
- mixed: bfloat16 [16, 4096, 2048], P('dp', 'sp')
All inputs are finite; a program needn't handle non-finite values.
Results may differ from a plain program's by a relative error of at most 0.01.
The roundings to bfloat16 on the way count: a program that leaves them out, or rounds other values in their place, can miss the bound.
Values may be sent and summed in bfloat16 or wider, within the bound.
No kernel may reach another device: no remote copies, remote signals or barrier semaphores. Data moves between devices by JAX's collectives and lax.ppermute only.
A program may use at most 128 MiB of HBM per device.

v0:
```python
import jax
import jax.numpy as jnp
from jax import lax
from jax.experimental import pallas as pl
from jax.experimental.pallas import tpu as pltpu
from jax.sharding import PartitionSpec as P


HEADS = 16
NOPE = 128
ROPE = 64
RANK = 512
ROWS = 256
SIDE = 4
LENGTH = 4096
LOCAL = HEADS // SIDE
PIECE = 144

EPSILON = 1e-06
THETA = 10000.0
LOG2E = 1.4426950408889634
SCALE2 = (NOPE + ROPE) ** (-0.5) * LOG2E
MIB = 2**20


f32 = jnp.float32
bf16 = jnp.bfloat16


PARTNER = [(d, d ^ 1) for d in range(16)]


def z_shift(k):
    return [(d, (d + 2 * k) % 16) for d in range(16)]


def z_blocks(w):
    blocks = [w] + [None] * 7
    ahead = behind = w
    for i in range(1, 4):
        ahead = lax.ppermute(ahead, "dp", z_shift(1))
        behind = lax.ppermute(behind, "dp", z_shift(-1))
        blocks[i] = ahead
        blocks[8 - i] = behind
    blocks[4] = lax.ppermute(ahead, "dp", z_shift(1))
    return jnp.concatenate(blocks, axis=0)


def y_shift(k):
    return [(s, (s + SIDE * k) % 16) for s in range(16)]


def x_shift(k):
    return [(s, (s // SIDE) * SIDE + (s % SIDE + k) % SIDE) for s in range(16)]


def limit(mib, **kw):
    return pltpu.CompilerParams(vmem_limit_bytes=mib * MIB, **kw)


SMEM = pl.BlockSpec(memory_space=pltpu.SMEM)
VMEM = pl.BlockSpec(memory_space=pltpu.VMEM)
ANY = pl.BlockSpec(memory_space=pl.ANY)


def normed(values, gain):
    scale = lax.rsqrt(jnp.mean(values * values, axis=-1, keepdims=True) + EPSILON)
    return values * scale * gain


def down_kernel(rows_ref, w_ref, gain_ref, rot_ref, a_ref, b_ref, q_ref):
    w = w_ref[...].reshape(2048, RANK)
    lat = jnp.dot(rows_ref[...], w, preferred_element_type=f32)
    lat = normed(lat, gain_ref[0]).astype(bf16)

    @pl.when(pl.program_id(0) == 0)
    def _():
        a_ref[0:128, :] = lat[0:128]
        a_ref[128:PIECE, :] = rot_ref[0]
        b_ref[0:128, :] = lat[128:256]
        b_ref[128:PIECE, :] = rot_ref[1]

    @pl.when(pl.program_id(0) == 1)
    def _():
        q_ref[...] = lat


def down(rows, w, gains, rot):
    piece = jax.ShapeDtypeStruct((PIECE, RANK), bf16)
    return pl.pallas_call(
        down_kernel,
        grid=(2,),
        in_specs=[
            pl.BlockSpec((ROWS, 2048), lambda n: (0, 0)),
            pl.BlockSpec((16, 1, 128, RANK), lambda n: (0, n, 0, 0)),
            pl.BlockSpec((1, 1, RANK), lambda n: (n, 0, 0)),
            pl.BlockSpec((2, 16, RANK), lambda n: (0, 0, 0)),
        ],
        out_specs=(
            pl.BlockSpec((PIECE, RANK), lambda n: (0, 0)),
            pl.BlockSpec((PIECE, RANK), lambda n: (0, 0)),
            pl.BlockSpec((ROWS, RANK), lambda n: (0, 0)),
        ),
        out_shape=(piece, piece, jax.ShapeDtypeStruct((ROWS, RANK), bf16)),
        compiler_params=limit(60, dimension_semantics=("arbitrary",)),
        name="down",
    )(rows, w, gains, rot)


def reader(low, high=None):
    def read(at, count):
        cut = low.shape[0]
        if at < cut:
            return low[at : at + count, :]
        return high[at - cut : at - cut + count, :]

    return read


def spot(yx_ref, i, j, half):
    at = ((yx_ref[0] - i + 4) % 4 * 4 + (yx_ref[1] - j + 4) % 4) * 256 + half * 128
    return pl.multiple_of(at, 128)


def expand(read, spots, w_ref, wvt_ref, k_ref, r_ref, vt_ref):
    rows = jnp.concatenate([read(PIECE * n, 128) for n in range(4)], axis=0)
    keys = jnp.dot(rows, w_ref[:, 0:512], preferred_element_type=f32).astype(bf16)
    values = lax.dot_general(
        wvt_ref[...], rows, (((1,), (1,)), ((), ())), preferred_element_type=f32
    ).astype(bf16)
    for n, at in enumerate(spots):
        for p in range(2):
            k_ref[p, pl.ds(at, 128), :] = keys[128 * n : 128 * n + 128, 256 * p : 256 * p + 256]
            vt_ref[p, :, pl.ds(at, 128)] = values[256 * p : 256 * p + 256, 128 * n : 128 * n + 128]
        packed = read(PIECE * n + 128, 16)
        rot = jnp.concatenate([packed[:, 64 * u : 64 * u + 64] for u in range(8)], axis=0)
        r_ref[pl.ds(at, 128), :] = jnp.concatenate([rot, jnp.zeros((128, 64), bf16)], axis=1)


def expand_queries(qn, i, w_ref, cos_ref, sin_ref, q_ref):
    both = jnp.dot(qn, w_ref[:, 1024:2048], preferred_element_type=f32)
    cosine = jnp.concatenate([cos_ref[:, 32 * i : 32 * i + 32]] * 8, axis=1)
    sine = jnp.concatenate([sin_ref[:, 32 * i : 32 * i + 32]] * 8, axis=1)
    turned = (both[:, 512:768] * cosine + both[:, 768:1024] * sine).astype(bf16)
    pad = jnp.zeros((ROWS, 64), bf16)
    for h in range(LOCAL):
        q_ref[h, ROWS * i : ROWS * (i + 1), 0:128] = both[:, 128 * h : 128 * h + 128].astype(bf16)
        q_ref[h, ROWS * i : ROWS * (i + 1), 128:256] = jnp.concatenate(
            [turned[:, 64 * h : 64 * h + 64], pad], axis=1
        )


COL = 4 * PIECE
ROW = COL + ROWS
UP = 32


def early_kernel(
    yx_ref, a0, a1, a3, b0, b1, b3, own_w, other_w, cos_ref, sin_ref,
    k_ref, r_ref, vt_ref, q_ref, w_ref, wvt_ref,
):
    z = yx_ref[2]
    core = yx_ref[3]
    for i in range(8):
        at = ((z - i + 8) % 8) * 2 * UP
        for ref, part in ((own_w, core), (other_w, 1 - core)):
            spot_at = pl.multiple_of(at + part * UP, UP)
            w_ref[pl.ds(spot_at, UP), :] = ref[UP * i : UP * (i + 1), :]
    wvt_ref[...] = w_ref[:, 512:1024].T
    outs = (w_ref, wvt_ref, k_ref, r_ref, vt_ref)
    for j, piece in ((0, a0), (1, a1), (3, a3)):
        expand(reader(piece), [spot(yx_ref, i, j, 0) for i in range(4)], *outs)
    for i, piece in ((0, b0), (1, b1), (3, b3)):
        expand(reader(piece), [spot(yx_ref, i, j, 1) for j in range(4)], *outs)
        expand_queries(piece[COL:ROW, :], i, w_ref, cos_ref, sin_ref, q_ref)


EXPANDED = (
    (2, LENGTH, 256),
    (LENGTH, 128),
    (2, 256, LENGTH),
    (LOCAL, SIDE * ROWS, 256),
)


def expand_early(yx, parts, w_own, w_other, cosine, sine):
    out = EXPANDED + ((RANK, 2048), (512, RANK))
    return pl.pallas_call(
        early_kernel,
        out_shape=tuple(jax.ShapeDtypeStruct(s, bf16) for s in out),
        in_specs=[SMEM] + [VMEM] * 10,
        out_specs=(VMEM,) * 6,
        compiler_params=limit(20),
        name="early",
    )(yx, *parts, w_own, w_other, cosine, sine)


KEYS = 512
PAIR = 2


def attend_kernel(
    yx_ref, a2l, a2h, b2l, b2h, cos_ref, sin_ref, k_in, r_in, vt_in, q_in, w_ref, wvt_ref,
    o0, o1, o2, o3, k_ref, r_ref, vt_ref, q_ref, score_ref, top_ref, sum_ref, acc_ref,
):
    pair = pl.program_id(0)
    step = pl.program_id(1)

    @pl.when((pair == 0) & (step == 0))
    def _():
        for p in range(2):
            k_ref[p] = k_in[p]
            vt_ref[p] = vt_in[p]
        r_ref[...] = r_in[...]
        for h in range(LOCAL):
            q_ref[h] = q_in[h]
        outs = (w_ref, wvt_ref, k_ref, r_ref, vt_ref)
        expand(reader(a2l, a2h), [spot(yx_ref, i, 2, 0) for i in range(4)], *outs)
        last = reader(b2l, b2h)
        expand(last, [spot(yx_ref, 2, j, 1) for j in range(4)], *outs)
        expand_queries(last(4 * PIECE, ROWS), 2, w_ref, cos_ref, sin_ref, q_ref)

    s = (yx_ref[0] - step + 4) % 4 * 4 + yx_ref[1]
    mine = pl.multiple_of(step * ROWS, ROWS)

    def score(at, slot, ahead):
        rot = r_ref[pl.ds(at, KEYS), :]
        for h in range(PAIR):
            keys = jnp.concatenate([k_ref[pair, pl.ds(at, KEYS), 128 * h : 128 * h + 128], rot], axis=1)
            query = q_ref[PAIR * pair + h, pl.ds(mine, ROWS), :]
            st = lax.dot_general(keys, query, (((1,), (1,)), ((), ())), preferred_element_type=f32)
            if ahead is not None:
                key_pos = lax.broadcasted_iota(jnp.int32, st.shape, 0)
                query_pos = lax.broadcasted_iota(jnp.int32, st.shape, 1)
                st = jnp.where(key_pos <= query_pos + ahead, st, -jnp.inf)
            score_ref[slot, h] = st

    def add(at, slot):
        for h in range(PAIR):
            st = score_ref[slot, h]
            top = top_ref[h]
            new = jnp.maximum(top, jnp.max(st, axis=0, keepdims=True))
            expo = jnp.exp2(st * SCALE2 - new * SCALE2)
            fade = jnp.exp2((top - new) * SCALE2)
            top_ref[h] = new
            sum_ref[h] = sum_ref[h] * fade + jnp.sum(expo, axis=0, keepdims=True)
            acc_ref[h] = acc_ref[h] * fade + jnp.dot(
                vt_ref[pair, 128 * h : 128 * h + 128, pl.ds(at, KEYS)],
                expo.astype(bf16),
                preferred_element_type=f32,
            )

    top_ref[...] = jnp.full(top_ref.shape, -jnp.inf, f32)
    sum_ref[...] = jnp.zeros(sum_ref.shape, f32)
    acc_ref[...] = jnp.zeros(acc_ref.shape, f32)
    full = s // 2
    last = pl.multiple_of(full * KEYS, KEYS)

    def at(j):
        return pl.multiple_of(j * KEYS, KEYS)

    def before(j):
        return pl.multiple_of(jnp.where(j == 0, full, j - 1) * KEYS, KEYS)

    score(last, 0, s * ROWS - last)

    def body(t, carry):
        j = 2 * t
        score(at(j), 1, None)
        add(before(j), 0)
        score(at(j + 1), 0, None)
        add(at(j), 1)
        return carry

    lax.fori_loop(0, full // 2, body, 0)

    @pl.when(full % 2 == 1)
    def _():
        score(at(full - 1), 1, None)
        add(before(full - 1), 0)
        add(at(full - 1), 1)

    @pl.when(full % 2 == 0)
    def _():
        add(before(full), 0)

    for i, o_ref in enumerate((o0, o1, o2, o3)):

        @pl.when(step == i)
        def _():
            for h in range(PAIR):
                o_ref[h * 128 : (h + 1) * 128, :] = (acc_ref[h] / sum_ref[h]).astype(bf16)


def attend(yx, halves, cosine, sine, early):
    piece = jax.ShapeDtypeStruct((LOCAL * 128, ROWS), bf16)
    return pl.pallas_call(
        attend_kernel,
        grid=(LOCAL // PAIR, SIDE),
        in_specs=[SMEM] + [VMEM] * 12,
        out_specs=(pl.BlockSpec((PAIR * 128, ROWS), lambda h, i: (h, 0)),) * SIDE,
        out_shape=(piece,) * SIDE,
        scratch_shapes=[pltpu.VMEM(s, bf16) for s in EXPANDED]
        + [
            pltpu.VMEM((2, PAIR, KEYS, ROWS), f32),
            pltpu.VMEM((PAIR, 1, ROWS), f32),
            pltpu.VMEM((PAIR, 1, ROWS), f32),
            pltpu.VMEM((PAIR, 128, ROWS), f32),
        ],
        compiler_params=limit(32, dimension_semantics=("arbitrary", "arbitrary")),
        name="attend",
    )(yx, *halves, cosine, sine, *early)


WIDE = 512


def out_kernel(y_ref, p0, p1, p2, p3, w_ref, gain_ref, o_ref, rows_ref, proj_ref):
    y = y_ref[0]
    for i, piece in enumerate((p0, p1, p2, p3)):
        g = pl.multiple_of(((y + i) % 4) * 512, 512)
        rows_ref[:, pl.ds(g, 512)] = piece[...].T
    for n in range(0, 2048, WIDE):
        proj_ref[:, n : n + WIDE] = jnp.dot(
            rows_ref[...], w_ref[:, n : n + WIDE], preferred_element_type=f32
        )
    o_ref[...] = normed(proj_ref[...], gain_ref[...]).astype(bf16)


def project(y, pieces, w_out, gain):
    return pl.pallas_call(
        out_kernel,
        in_specs=[SMEM] + [VMEM] * 6,
        out_specs=VMEM,
        out_shape=jax.ShapeDtypeStruct((ROWS, 2048), bf16),
        scratch_shapes=[pltpu.VMEM((ROWS, 2048), bf16), pltpu.VMEM((ROWS, 2048), f32)],
        compiler_params=limit(16),
        name="project",
    )(y, *pieces, w_out, gain)


def stage_kernel(w_ref, o_ref, sem):
    copy = pltpu.make_async_copy(w_ref, o_ref, sem)
    copy.start()
    copy.wait()


def stage(w):
    return pl.pallas_call(
        stage_kernel,
        in_specs=[ANY],
        out_specs=VMEM,
        out_shape=jax.ShapeDtypeStruct(w.shape, w.dtype),
        scratch_shapes=[pltpu.SemaphoreType.DMA],
        compiler_params=limit(16),
        name="stage",
    )(w)


def up_columns(w_qup, w_kvup, y):
    rows = w_qup.shape[0]
    q = lax.dynamic_slice_in_dim(w_qup, y * LOCAL * 192, LOCAL * 192, 1).reshape(rows, LOCAL, 192)
    kv = lax.dynamic_slice_in_dim(w_kvup, y * LOCAL * 256, LOCAL * 256, 1).reshape(rows, LOCAL, 256)
    first = q[..., 128:160]
    second = q[..., 160:192]
    parts = [
        kv[..., :128],
        kv[..., 128:],
        q[..., :128],
        jnp.concatenate([first, second], axis=-1),
        jnp.concatenate([-second, first], axis=-1),
    ]
    return jnp.concatenate([p.reshape(rows, -1) for p in parts], axis=1)


def body(tokens, w_qdown, w_kvdown, w_rotary, q_gain, kv_gain, w_qup, w_kvup, w_out, out_gain):
    sp_place = lax.axis_index("sp")
    y = sp_place // SIDE
    x = sp_place % SIDE
    own = tokens[0]
    w_down = lax.all_gather(jnp.stack([w_kvdown, w_qdown]), "dp")

    lanes = jnp.arange(SIDE * 32)
    spots = ((y - lanes // 32 + SIDE) % SIDE) * SIDE + x
    positions = (spots[None, :] * ROWS + jnp.arange(ROWS)[:, None]).astype(f32)
    freqs = THETA ** (-(2 * (lanes % 32)).astype(f32) / ROPE)
    angles = positions * freqs[None, :]
    cosine = jnp.cos(angles)
    sine = jnp.sin(angles)

    turned = jnp.dot(own, w_rotary, preferred_element_type=f32)
    first = turned[:, :32]
    second = turned[:, 32:]
    cos_own = cosine[:, :32]
    sin_own = sine[:, :32]
    key_rot = jnp.concatenate(
        [first * cos_own - second * sin_own, second * cos_own + first * sin_own], axis=-1
    ).astype(bf16)
    packed = key_rot.reshape(2, 8, 16, 64).transpose(0, 2, 1, 3).reshape(2, 16, 512)

    w_own = z_blocks(up_columns(w_qup, w_kvup, y))
    w_other = lax.ppermute(w_own, "dp", PARTNER)
    dp_place = lax.axis_index("dp")
    yx = jnp.stack([y, x, dp_place // 2, dp_place % 2])
    w_down, w_own, w_other, cosine, sine, packed, yx = lax.optimization_barrier(
        (w_down, w_own, w_other, cosine, sine, packed, yx)
    )
    w_full = lax.all_gather(w_out, "dp", axis=1, tiled=True)

    gains = jnp.stack([kv_gain, q_gain]).reshape(2, 1, RANK)
    a, b, qn = down(own, w_down, gains, packed)

    b1, b2, b3 = (lax.ppermute(b, "sp", x_shift(k)) for k in (1, 2, 3))
    a1, a2, a3 = (lax.ppermute(a, "sp", y_shift(k)) for k in (1, 2, 3))
    col = jnp.concatenate([a, a1, a2, a3], axis=0)
    row = jnp.concatenate([b, b1, b2, b3, qn], axis=0)
    col1 = lax.ppermute(col, "sp", x_shift(1))
    col3 = lax.ppermute(col, "sp", x_shift(-1))
    row1 = lax.ppermute(row, "sp", y_shift(1))
    row3 = lax.ppermute(row, "sp", y_shift(-1))
    col2l = lax.ppermute(col1[:288], "sp", x_shift(1))
    col2h = lax.ppermute(col3[288:], "sp", x_shift(-1))
    row2l = lax.ppermute(row1[:416], "sp", y_shift(1))
    row2h = lax.ppermute(row3[416:], "sp", y_shift(-1))

    early = expand_early(
        yx, (col, col1, col3, row, row1, row3), w_own, w_other, cosine, sine
    )
    attended = attend(yx, (col2l, col2h, row2l, row2h), cosine, sine, early)
    w_full, *attended = lax.optimization_barrier((w_full, *attended))
    pieces = [attended[0]] + [
        lax.ppermute(attended[i], "sp", y_shift(-i)) for i in range(1, SIDE)
    ]
    mixed = project(y.reshape(1), pieces, stage(w_full), out_gain.reshape(1, 2048))
    return mixed[None]


def solution(mesh):
    in_specs = (
        P("dp", "sp", None),
        P("dp", None),
        P("dp", None),
        P(),
        P(),
        P(),
        P("dp", None),
        P("dp", None),
        P(None, "dp"),
        P(),
    )
    out_specs = P("dp", "sp", None)

    return jax.shard_map(body, mesh=mesh, in_specs=in_specs, out_specs=out_specs, check_vma=False)
```

profile of v0, /device:TPU:6, one launch (start us, length us, event | category | flops | bytes accessed | tf_op | source)
XLA Modules:
  0.0 170.9 jit_solution(4283518948019950140)
XLA Ops:
  12.7 4.0 %collective-permute-start.4 = (bf16[32,2048]{1,0:T(8,128)(2,1)S(1)}, bf16[32,2048]{1,0:T(8,128)(2,1)S(1)}, u32[]{:S(2)}, u32[]{:S(2)}) collective-permute-start(bf16[32,2048]{1,0:T(8,128)(2,1)S(1)} %get-tuple-element.67), channel_id=1, source_target_pairs={{0,14},{1,15},{2,0},{3,1},{4,2},{5,3},{6,4},{7,5},{8,6},{9,7},{10,... | collective-permute-start | bytes 393224 | tf_op jit(solution)/shard_map/ppermute | solution.py:42
  16.7 3.4 %collective-permute-done = bf16[32,2048]{1,0:T(8,128)(2,1)S(1)} collective-permute-done((bf16[32,2048]{1,0:T(8,128)(2,1)S(1)}, bf16[32,2048]{1,0:T(8,128)(2,1)S(1)}, u32[]{:S(2)}, u32[]{:S(2)}) %collective-permute-start) | collective-permute-done | bytes 131104 | tf_op jit(solution)/shard_map/ppermute | solution.py:41
  20.1 3.2 %collective-permute-start.5 = (bf16[32,2048]{1,0:T(8,128)(2,1)S(1)}, bf16[32,2048]{1,0:T(8,128)(2,1)S(1)}, u32[]{:S(2)}, u32[]{:S(2)}) collective-permute-start(bf16[32,2048]{1,0:T(8,128)(2,1)S(1)} %collective-permute-done.4), channel_id=1, source_target_pairs={{0,14},{1,15},{2,0},{3,1},{4,2},{5,3},{6,4},{7,5},{8,6},{9,7},{10,... | collective-permute-start | bytes 393224 | tf_op jit(solution)/shard_map/ppermute | solution.py:42
  23.4 2.9 %collective-permute-done.1 = bf16[32,2048]{1,0:T(8,128)(2,1)S(1)} collective-permute-done((bf16[32,2048]{1,0:T(8,128)(2,1)S(1)}, bf16[32,2048]{1,0:T(8,128)(2,1)S(1)}, u32[]{:S(2)}, u32[]{:S(2)}) %collective-permute-start.1) | collective-permute-done | bytes 131104 | tf_op jit(solution)/shard_map/ppermute | solution.py:41
  28.3 3.7 %collective-permute-start.6 = (bf16[32,2048]{1,0:T(8,128)(2,1)S(1)}, bf16[32,2048]{1,0:T(8,128)(2,1)S(1)}, u32[]{:S(2)}, u32[]{:S(2)}) collective-permute-start(bf16[32,2048]{1,0:T(8,128)(2,1)S(1)} %collective-permute-done.5), channel_id=1, source_target_pairs={{0,14},{1,15},{2,0},{3,1},{4,2},{5,3},{6,4},{7,5},{8,6},{9,7},{10,... | collective-permute-start | bytes 393224 | tf_op jit(solution)/shard_map/ppermute | solution.py:42
  32.0 3.4 %collective-permute-done.2 = bf16[32,2048]{1,0:T(8,128)(2,1)S(1)} collective-permute-done((bf16[32,2048]{1,0:T(8,128)(2,1)S(1)}, bf16[32,2048]{1,0:T(8,128)(2,1)S(1)}, u32[]{:S(2)}, u32[]{:S(2)}) %collective-permute-start.2) | collective-permute-done | bytes 131104 | tf_op jit(solution)/shard_map/ppermute | solution.py:41
  35.5 8.9 %collective-permute-done.3 = bf16[32,2048]{1,0:T(8,128)(2,1)S(1)} collective-permute-done((bf16[32,2048]{1,0:T(8,128)(2,1)S(1)}, bf16[32,2048]{1,0:T(8,128)(2,1)S(1)}, u32[]{:S(2)}, u32[]{:S(2)}) %collective-permute-start.3) | collective-permute-done | bytes 131104 | tf_op jit(solution)/shard_map/ppermute | solution.py:45
  48.4 8.3 %all-gather.6.cloned.1.call-done = bf16[32,128,512]{2,1,0:T(8,128)(2,1)} async-done(((bf16[2,128,512]{2,1,0:T(8,128)(2,1)}), bf16[32,128,512]{2,1,0:T(8,128)(2,1)}) %all-gather.6.cloned.1.call-update) | async-done | bytes 4194320 | tf_op jit(solution)/shard_map/all_gather | solution.py:381
  56.7 4.4 %down.1 = (bf16[144,512]{1,0:T(8,128)(2,1)}, bf16[144,512]{1,0:T(8,128)(2,1)}, bf16[256,512]{1,0:T(8,128)(2,1)}) custom-call(bf16[256,2048]{1,0:T(8,128)(2,1)} %bitcast.35, bf16[16,2,128,512]{3,2,1,0:T(8,128)(2,1)} %bitcast.34, f32[2,1,512]{2,1,0:T(1,128)} %reshape.91.gain_ref, bf16[2,16,512]{2,1,0:T(8,128)(2,1)} %reshape.90.rot_ref), custom_call_target="tpu_custom_call" | custom-call | tf_op jit(solution)/shard_map/down/pallas_call | solution.py:90
  61.5 2.4 %collective-permute-start.16 = (bf16[144,512]{1,0:T(8,128)(2,1)}, bf16[144,512]{1,0:T(8,128)(2,1)S(1)}, u32[]{:S(2)}, u32[]{:S(2)}) collective-permute-start(bf16[144,512]{1,0:T(8,128)(2,1)} %get-tuple-element.34), channel_id=1, source_target_pairs={{0,32},{16,48},{32,0},{48,16},{64,96},{80,112},{96,64},{112,80},{1... | collective-permute-start | bytes 442376 | tf_op jit(solution)/shard_map/ppermute | solution.py:413
  66.5 3.2 %collective-permute-start.9 = (bf16[144,512]{1,0:T(8,128)(2,1)}, bf16[144,512]{1,0:T(8,128)(2,1)S(1)}, u32[]{:S(2)}, u32[]{:S(2)}) collective-permute-start(bf16[144,512]{1,0:T(8,128)(2,1)} %get-tuple-element.33), channel_id=1, source_target_pairs={{0,128},{16,144},{32,160},{48,176},{64,192},{80,208},{96,224},{112... | collective-permute-start | bytes 442376 | tf_op jit(solution)/shard_map/ppermute | solution.py:414
  69.7 2.4 %collective-permute-done.17 = bf16[144,512]{1,0:T(8,128)(2,1)S(1)} collective-permute-done((bf16[144,512]{1,0:T(8,128)(2,1)}, bf16[144,512]{1,0:T(8,128)(2,1)S(1)}, u32[]{:S(2)}, u32[]{:S(2)}) %collective-permute-start.17) | collective-permute-done | bytes 147488 | tf_op jit(solution)/shard_map/ppermute | solution.py:413
  74.7 2.0 %collective-permute-start.20 = (bf16[832,512]{1,0:T(8,128)(2,1)S(1)}, bf16[832,512]{1,0:T(8,128)(2,1)S(1)}, u32[]{:S(2)}, u32[]{:S(2)}) collective-permute-start(bf16[832,512]{1,0:T(8,128)(2,1)S(1)} %constant_dynamic-update-slice_fusion.21.b0), channel_id=1, source_target_pairs={{0,192},{16,208},{32,224},{48,240},{64,0},{80,16},{96,32},{112,48}... | collective-permute-start | bytes 2555912 | tf_op jit(solution)/shard_map/ppermute | solution.py:420
  79.7 18.3 %collective-permute-done.10 = bf16[144,512]{1,0:T(8,128)(2,1)S(1)} collective-permute-done((bf16[144,512]{1,0:T(8,128)(2,1)}, bf16[144,512]{1,0:T(8,128)(2,1)S(1)}, u32[]{:S(2)}, u32[]{:S(2)}) %collective-permute-start.10) | collective-permute-done | bytes 147488 | tf_op jit(solution)/shard_map/ppermute | solution.py:414
  103.6 8.3 %collective-permute-done.11.a1 = bf16[576,512]{1,0:T(8,128)(2,1)S(1)} collective-permute-done((bf16[576,512]{1,0:T(8,128)(2,1)S(1)}, bf16[576,512]{1,0:T(8,128)(2,1)S(1)}, u32[]{:S(2)}, u32[]{:S(2)}) %collective-permute-start.11) | collective-permute-done | bytes 589856 | tf_op jit(solution)/shard_map/ppermute | solution.py:417
  112.0 2.2 %collective-permute-start.12 = (bf16[288,512]{1,0:T(8,128)(2,1)S(1)}, bf16[288,512]{1,0:T(8,128)(2,1)S(1)}, u32[]{:S(2)}, u32[]{:S(2)}) collective-permute-start(bf16[288,512]{1,0:T(8,128)(2,1)S(1)} %slice.62), channel_id=1, source_target_pairs={{0,16},{16,32},{32,48},{48,0},{64,80},{80,96},{96,112},{112,64},{1... | collective-permute-start | bytes 884744 | tf_op jit(solution)/shard_map/ppermute | solution.py:421
  114.3 5.8 %early.1 = (bf16[2,4096,256]{2,1,0:T(8,128)(2,1)S(1)}, bf16[4096,128]{1,0:T(8,128)(2,1)S(1)}, bf16[2,256,4096]{2,1,0:T(8,128)(2,1)S(1)}, bf16[4,1024,256]{2,1,0:...) custom-call(s32[4]{0:T(128)S(1)} %pad_add_fusion.yx_ref, ...), custom_call_target="tpu_custom_call" | custom-call | tf_op jit(solution)/shard_map/early/pallas_call | solution.py:188
  120.1 2.1 %collective-permute-done.14.a2h = bf16[288,512]{1,0:T(8,128)(2,1)S(1)} collective-permute-done((bf16[288,512]{1,0:T(8,128)(2,1)S(1)}, bf16[288,512]{1,0:T(8,128)(2,1)S(1)}, u32[]{:S(2)}, u32[]{:S(2)}) %collective-permute-start.14) | collective-permute-done | bytes 294944 | tf_op jit(solution)/shard_map/ppermute | solution.py:422
  122.2 21.7 %attend.1 = (bf16[512,256]{1,0:T(8,128)(2,1)S(1)}, bf16[512,256]{1,0:T(8,128)(2,1)S(1)}, bf16[512,256]{1,0:T(8,128)(2,1)S(1)}, bf16[512,256]{1,0:T(8,128)(2,1)S(1)}) custom-call(s32[4]{0:T(128)S(1)} %pad_add_fusion.yx_ref, bf16[288,512]{1,0:T(8,128)(2,1)S(1)} %collective-permute-done.12.a2l, bf16[288,512]{1,0:T(8,128)(2,1)S(1)} %collective-permute-done.14.a2h, ...), custom_call_target="tpu_custom_call" | custom-call | tf_op jit(solution)/shard_map/attend/pallas_call | solution.py:297
  143.9 4.0 %collective-permute-start.22 = (bf16[512,256]{1,0:T(8,128)(2,1)S(1)}, bf16[512,256]{1,0:T(8,128)(2,1)S(1)}, u32[]{:S(2)}, u32[]{:S(2)}) collective-permute-start(bf16[512,256]{1,0:T(8,128)(2,1)S(1)} %get-tuple-element.51), channel_id=1, source_target_pairs={{0,192},{16,208},{32,224},{48,240},{64,0},{80,16},{96,32},{112,48}... | collective-permute-start | bytes 786440 | tf_op jit(solution)/shard_map/ppermute | solution.py:432
  148.9 3.4 %copy-done.1 = bf16[2048,2048]{1,0:T(8,128)(2,1)S(1)} copy-done((bf16[2048,2048]{1,0:T(8,128)(2,1)S(1)}, bf16[2048,2048]{1,0:T(8,128)(2,1)}, u32[]{:S(2)}) %copy-start.1) | copy-done | bytes 8388632
  152.9 3.9 %collective-permute-done.22.p1 = bf16[512,256]{1,0:T(8,128)(2,1)S(1)} collective-permute-done((bf16[512,256]{1,0:T(8,128)(2,1)S(1)}, bf16[512,256]{1,0:T(8,128)(2,1)S(1)}, u32[]{:S(2)}, u32[]{:S(2)}) %collective-permute-start.22) | collective-permute-done | bytes 262176 | tf_op jit(solution)/shard_map/ppermute | solution.py:432
  157.7 2.5 %collective-permute-done.24.p3 = bf16[512,256]{1,0:T(8,128)(2,1)S(1)} collective-permute-done((bf16[512,256]{1,0:T(8,128)(2,1)S(1)}, bf16[512,256]{1,0:T(8,128)(2,1)S(1)}, u32[]{:S(2)}, u32[]{:S(2)}) %collective-permute-start.24) | collective-permute-done | bytes 262176 | tf_op jit(solution)/shard_map/ppermute | solution.py:432
  160.2 3.8 %project.1 = bf16[256,2048]{1,0:T(8,128)(2,1)} custom-call(s32[1]{0:T(128)} %bitcast.y_ref, bf16[512,256]{1,0:T(8,128)(2,1)S(1)} %get-tuple-element.50.p0, bf16[512,256]{1,0:T(8,128)(2,1)S(1)} %collective-permute-done.22.p1, bf16[512,256]{1,0:T(8,128)(2,1)S(1)} %collective-permute-done.23.p2, bf16[512,256]{1,0:T(8,128)(2,1)S(1)} %collective-permute-done.24.p3, ...), custom_call_target="tpu_custom_call" | custom-call | tf_op jit(solution)/shard_map/project/pallas_call | solution.py:331
  (97 shorter events, 28.8 us)
Async XLA Ops:
  6.5 50.1 %all-gather.6.cloned.1.call-start = ((), (), s32[]{:S(2)}) async-start(), calls=%async_computation.1 | async-start | bytes 4456448 | tf_op jit(solution)/shard_map/all_gather | solution.py:381
  8.4 135.6 %all-gather.4.cloned.1.call-start = ((), (), s32[]{:S(2)}) async-start(), calls=%async_computation | async-start | bytes 8912896 | tf_op jit(solution)/shard_map/all_gather | solution.py:408
  10.7 9.4 %collective-permute-start = (bf16[32,2048]{1,0:T(8,128)(2,1)S(1)}, bf16[32,2048]{1,0:T(8,128)(2,1)S(1)}, u32[]{:S(2)}, u32[]{:S(2)}) collective-permute-start(bf16[32,2048]{1,0:T(8,128)(2,1)S(1)} %get-tuple-element.67), channel_id=1, source_target_pairs={{0,2},{1,3},{2,4},{3,5},{4,6},{5,7},{6,8},{7,9},{8,10},{9,11},{10,... | collective-permute-start | bytes 393224 | tf_op jit(solution)/shard_map/ppermute | solution.py:41
  12.7 7.4 %collective-permute-start.4 = (bf16[32,2048]{1,0:T(8,128)(2,1)S(1)}, bf16[32,2048]{1,0:T(8,128)(2,1)S(1)}, u32[]{:S(2)}, u32[]{:S(2)}) collective-permute-start(bf16[32,2048]{1,0:T(8,128)(2,1)S(1)} %get-tuple-element.67), channel_id=1, source_target_pairs={{0,14},{1,15},{2,0},{3,1},{4,2},{5,3},{6,4},{7,5},{8,6},{9,7},{10,... | collective-permute-start | bytes 393224 | tf_op jit(solution)/shard_map/ppermute | solution.py:42
  20.1 8.2 %collective-permute-start.5 = (bf16[32,2048]{1,0:T(8,128)(2,1)S(1)}, bf16[32,2048]{1,0:T(8,128)(2,1)S(1)}, u32[]{:S(2)}, u32[]{:S(2)}) collective-permute-start(bf16[32,2048]{1,0:T(8,128)(2,1)S(1)} %collective-permute-done.4), channel_id=1, source_target_pairs={{0,14},{1,15},{2,0},{3,1},{4,2},{5,3},{6,4},{7,5},{8,6},{9,7},{10,... | collective-permute-start | bytes 393224 | tf_op jit(solution)/shard_map/ppermute | solution.py:42
  26.3 9.1 %collective-permute-start.2 = (bf16[32,2048]{1,0:T(8,128)(2,1)S(1)}, bf16[32,2048]{1,0:T(8,128)(2,1)S(1)}, u32[]{:S(2)}, u32[]{:S(2)}) collective-permute-start(bf16[32,2048]{1,0:T(8,128)(2,1)S(1)} %collective-permute-done.1), channel_id=1, source_target_pairs={{0,2},{1,3},{2,4},{3,5},{4,6},{5,7},{6,8},{7,9},{8,10},{9,11},{10,... | collective-permute-start | bytes 393224 | tf_op jit(solution)/shard_map/ppermute | solution.py:41
  28.3 16.1 %collective-permute-start.6 = (bf16[32,2048]{1,0:T(8,128)(2,1)S(1)}, bf16[32,2048]{1,0:T(8,128)(2,1)S(1)}, u32[]{:S(2)}, u32[]{:S(2)}) collective-permute-start(bf16[32,2048]{1,0:T(8,128)(2,1)S(1)} %collective-permute-done.5), channel_id=1, source_target_pairs={{0,14},{1,15},{2,0},{3,1},{4,2},{5,3},{6,4},{7,5},{8,6},{9,7},{10,... | collective-permute-start | bytes 393224 | tf_op jit(solution)/shard_map/ppermute | solution.py:42
  35.4 9.0 %collective-permute-start.3 = (bf16[32,2048]{1,0:T(8,128)(2,1)S(1)}, bf16[32,2048]{1,0:T(8,128)(2,1)S(1)}, u32[]{:S(2)}, u32[]{:S(2)}) collective-permute-start(bf16[32,2048]{1,0:T(8,128)(2,1)S(1)} %collective-permute-done.2), channel_id=1, source_target_pairs={{0,2},{1,3},{2,4},{3,5},{4,6},{5,7},{6,8},{7,9},{8,10},{9,11},{10,... | collective-permute-start | bytes 393224 | tf_op jit(solution)/shard_map/ppermute | solution.py:45
  61.0 8.7 %collective-permute-start.15 = (bf16[144,512]{1,0:T(8,128)(2,1)}, bf16[144,512]{1,0:T(8,128)(2,1)S(1)}, u32[]{:S(2)}, u32[]{:S(2)}) collective-permute-start(bf16[144,512]{1,0:T(8,128)(2,1)} %get-tuple-element.34), channel_id=1, source_target_pairs={{0,16},{16,32},{32,48},{48,0},{64,80},{80,96},{96,112},{112,64},{1... | collective-permute-start | bytes 442376 | tf_op jit(solution)/shard_map/ppermute | solution.py:413
  61.5 8.2 %collective-permute-start.16 = (bf16[144,512]{1,0:T(8,128)(2,1)}, bf16[144,512]{1,0:T(8,128)(2,1)S(1)}, u32[]{:S(2)}, u32[]{:S(2)}) collective-permute-start(bf16[144,512]{1,0:T(8,128)(2,1)} %get-tuple-element.34), channel_id=1, source_target_pairs={{0,32},{16,48},{32,0},{48,16},{64,96},{80,112},{96,64},{112,80},{1... | collective-permute-start | bytes 442376 | tf_op jit(solution)/shard_map/ppermute | solution.py:413
  65.0 14.7 %collective-permute-start.8 = (bf16[144,512]{1,0:T(8,128)(2,1)}, bf16[144,512]{1,0:T(8,128)(2,1)S(1)}, u32[]{:S(2)}, u32[]{:S(2)}) collective-permute-start(bf16[144,512]{1,0:T(8,128)(2,1)} %get-tuple-element.33), channel_id=1, source_target_pairs={{0,64},{16,80},{32,96},{48,112},{64,128},{80,144},{96,160},{112,17... | collective-permute-start | bytes 442376 | tf_op jit(solution)/shard_map/ppermute | solution.py:414
  66.5 13.2 %collective-permute-start.9 = (bf16[144,512]{1,0:T(8,128)(2,1)}, bf16[144,512]{1,0:T(8,128)(2,1)S(1)}, u32[]{:S(2)}, u32[]{:S(2)}) collective-permute-start(bf16[144,512]{1,0:T(8,128)(2,1)} %get-tuple-element.33), channel_id=1, source_target_pairs={{0,128},{16,144},{32,160},{48,176},{64,192},{80,208},{96,224},{112... | collective-permute-start | bytes 442376 | tf_op jit(solution)/shard_map/ppermute | solution.py:414
  73.1 27.1 %collective-permute-start.18 = (bf16[832,512]{1,0:T(8,128)(2,1)S(1)}, bf16[832,512]{1,0:T(8,128)(2,1)S(1)}, u32[]{:S(2)}, u32[]{:S(2)}) collective-permute-start(bf16[832,512]{1,0:T(8,128)(2,1)S(1)} %constant_dynamic-update-slice_fusion.21.b0), channel_id=1, source_target_pairs={{0,64},{16,80},{32,96},{48,112},{64,128},{80,144},{96,160},{112,17... | collective-permute-start | bytes 2555912 | tf_op jit(solution)/shard_map/ppermute | solution.py:419
  74.7 27.3 %collective-permute-start.20 = (bf16[832,512]{1,0:T(8,128)(2,1)S(1)}, bf16[832,512]{1,0:T(8,128)(2,1)S(1)}, u32[]{:S(2)}, u32[]{:S(2)}) collective-permute-start(bf16[832,512]{1,0:T(8,128)(2,1)S(1)} %constant_dynamic-update-slice_fusion.21.b0), channel_id=1, source_target_pairs={{0,192},{16,208},{32,224},{48,240},{64,0},{80,16},{96,32},{112,48}... | collective-permute-start | bytes 2555912 | tf_op jit(solution)/shard_map/ppermute | solution.py:420
  77.7 20.4 %collective-permute-start.10 = (bf16[144,512]{1,0:T(8,128)(2,1)}, bf16[144,512]{1,0:T(8,128)(2,1)S(1)}, u32[]{:S(2)}, u32[]{:S(2)}) collective-permute-start(bf16[144,512]{1,0:T(8,128)(2,1)} %get-tuple-element.33), channel_id=1, source_target_pairs={{0,192},{16,208},{32,224},{48,240},{64,0},{80,16},{96,32},{112,48}... | collective-permute-start | bytes 442376 | tf_op jit(solution)/shard_map/ppermute | solution.py:414
  98.1 13.9 %collective-permute-start.11 = (bf16[576,512]{1,0:T(8,128)(2,1)S(1)}, bf16[576,512]{1,0:T(8,128)(2,1)S(1)}, u32[]{:S(2)}, u32[]{:S(2)}) collective-permute-start(bf16[576,512]{1,0:T(8,128)(2,1)S(1)} %constant_dynamic-update-slice_fusion.17.a0), channel_id=1, source_target_pairs={{0,16},{16,32},{32,48},{48,0},{64,80},{80,96},{96,112},{112,64},{1... | collective-permute-start | bytes 1769480 | tf_op jit(solution)/shard_map/ppermute | solution.py:417
  99.2 15.0 %collective-permute-start.13 = (bf16[576,512]{1,0:T(8,128)(2,1)S(1)}, bf16[576,512]{1,0:T(8,128)(2,1)S(1)}, u32[]{:S(2)}, u32[]{:S(2)}) collective-permute-start(bf16[576,512]{1,0:T(8,128)(2,1)S(1)} %constant_dynamic-update-slice_fusion.17.a0), channel_id=1, source_target_pairs={{0,48},{16,0},{32,16},{48,32},{64,112},{80,64},{96,80},{112,96},{1... | collective-permute-start | bytes 1769480 | tf_op jit(solution)/shard_map/ppermute | solution.py:418
  100.2 22.0 %collective-permute-start.19 = (bf16[416,512]{1,0:T(8,128)(2,1)S(1)}, bf16[416,512]{1,0:T(8,128)(2,1)S(1)}, u32[]{:S(2)}, u32[]{:S(2)}) collective-permute-start(bf16[416,512]{1,0:T(8,128)(2,1)S(1)} %slice.64), channel_id=1, source_target_pairs={{0,64},{16,80},{32,96},{48,112},{64,128},{80,144},{96,160},{112,17... | collective-permute-start | bytes 1277960 | tf_op jit(solution)/shard_map/ppermute | solution.py:423
  102.1 20.1 %collective-permute-start.21 = (bf16[416,512]{1,0:T(8,128)(2,1)S(1)}, bf16[416,512]{1,0:T(8,128)(2,1)S(1)}, u32[]{:S(2)}, u32[]{:S(2)}) collective-permute-start(bf16[416,512]{1,0:T(8,128)(2,1)S(1)} %slice.65), channel_id=1, source_target_pairs={{0,192},{16,208},{32,224},{48,240},{64,0},{80,16},{96,32},{112,48}... | collective-permute-start | bytes 1277960 | tf_op jit(solution)/shard_map/ppermute | solution.py:424
  112.0 8.1 %collective-permute-start.12 = (bf16[288,512]{1,0:T(8,128)(2,1)S(1)}, bf16[288,512]{1,0:T(8,128)(2,1)S(1)}, u32[]{:S(2)}, u32[]{:S(2)}) collective-permute-start(bf16[288,512]{1,0:T(8,128)(2,1)S(1)} %slice.62), channel_id=1, source_target_pairs={{0,16},{16,32},{32,48},{48,0},{64,80},{80,96},{96,112},{112,64},{1... | collective-permute-start | bytes 884744 | tf_op jit(solution)/shard_map/ppermute | solution.py:421
  114.2 8.0 %collective-permute-start.14 = (bf16[288,512]{1,0:T(8,128)(2,1)S(1)}, bf16[288,512]{1,0:T(8,128)(2,1)S(1)}, u32[]{:S(2)}, u32[]{:S(2)}) collective-permute-start(bf16[288,512]{1,0:T(8,128)(2,1)S(1)} %slice.63), channel_id=1, source_target_pairs={{0,48},{16,0},{32,16},{48,32},{64,112},{80,64},{96,80},{112,96},{1... | collective-permute-start | bytes 884744 | tf_op jit(solution)/shard_map/ppermute | solution.py:422
  143.9 12.8 %collective-permute-start.22 = (bf16[512,256]{1,0:T(8,128)(2,1)S(1)}, bf16[512,256]{1,0:T(8,128)(2,1)S(1)}, u32[]{:S(2)}, u32[]{:S(2)}) collective-permute-start(bf16[512,256]{1,0:T(8,128)(2,1)S(1)} %get-tuple-element.51), channel_id=1, source_target_pairs={{0,192},{16,208},{32,224},{48,240},{64,0},{80,16},{96,32},{112,48}... | collective-permute-start | bytes 786440 | tf_op jit(solution)/shard_map/ppermute | solution.py:432
  148.0 9.7 %collective-permute-start.23 = (bf16[512,256]{1,0:T(8,128)(2,1)S(1)}, bf16[512,256]{1,0:T(8,128)(2,1)S(1)}, u32[]{:S(2)}, u32[]{:S(2)}) collective-permute-start(bf16[512,256]{1,0:T(8,128)(2,1)S(1)} %get-tuple-element.52), channel_id=1, source_target_pairs={{0,128},{16,144},{32,160},{48,176},{64,192},{80,208},{96,224},{112... | collective-permute-start | bytes 786440 | tf_op jit(solution)/shard_map/ppermute | solution.py:432
  148.0 12.2 %collective-permute-start.24 = (bf16[512,256]{1,0:T(8,128)(2,1)S(1)}, bf16[512,256]{1,0:T(8,128)(2,1)S(1)}, u32[]{:S(2)}, u32[]{:S(2)}) collective-permute-start(bf16[512,256]{1,0:T(8,128)(2,1)S(1)} %get-tuple-element.53), channel_id=1, source_target_pairs={{0,64},{16,80},{32,96},{48,112},{64,128},{80,144},{96,160},{112,17... | collective-permute-start | bytes 786440 | tf_op jit(solution)/shard_map/ppermute | solution.py:432
  (9 other events, 153.0 us)
Sparse Core Ops, SparseCore 0:
  9.2 47.4 all-gather.5
  58.4 62.6 all-gather.3
where the time goes:
time: 171 us
  waiting for transfers between devices  68.1 us (40%)
  starting transfers between devices  39.2 us (23%)
  Pallas kernels  36.3 us (21%)
  between operations  13.8 us (8%)
  local copies, waits for them, and re-layouts  9.08 us (5%)
  other arithmetic  2.73 us (2%)
    pallas_call x1, Pallas kernels, attend(): pl.pallas_call(attend_kernel, grid=(LOCAL // PAIR, SIDE), in_specs=[SMEM]...  21.7 us
    ppermute x3, waiting for transfers between devices, body(): a1, a2, a3 = (lax.ppermute(a, 'sp', y_shift(k)) for k in (1, 2, 3))  18.3 us
    ppermute x3, starting transfers between devices, z_blocks(): behind = lax.ppermute(behind, 'dp', z_shift(-1))  11 us
    ppermute x3, waiting for transfers between devices, z_blocks(): ahead = lax.ppermute(ahead, 'dp', z_shift(1))  9.74 us
    ppermute x1, waiting for transfers between devices, z_blocks(): blocks[4] = lax.ppermute(ahead, 'dp', z_shift(1))  8.94 us
    ppermute x1, waiting for transfers between devices, body(): col1 = lax.ppermute(col, 'sp', x_shift(1))  8.32 us
    all_gather x1, waiting for transfers between devices, body(): w_down = lax.all_gather(jnp.stack([w_kvdown, w_qdown]), 'dp')  8.27 us
    ppermute x3, waiting for transfers between devices, body(): lax.ppermute(attended[i], 'sp', y_shift(-i))  7.29 us
  transfers between devices with their start and end apart: 27, of which 13 were waited for; matrix products, arithmetic and copies ran while one was open for 5% of the time, Pallas kernels for 19%

commit v1 on v0

--- a/solution.py
+++ b/solution.py
@@ -68,43 +68,42 @@
     return values * scale * gain
 
 
-def down_kernel(rows_ref, w_ref, gain_ref, rot_ref, a_ref, b_ref, q_ref):
+def latent(rows_ref, w_ref, gain_ref):
     w = w_ref[...].reshape(2048, RANK)
     lat = jnp.dot(rows_ref[...], w, preferred_element_type=f32)
-    lat = normed(lat, gain_ref[0]).astype(bf16)
-
-    @pl.when(pl.program_id(0) == 0)
-    def _():
-        a_ref[0:128, :] = lat[0:128]
-        a_ref[128:PIECE, :] = rot_ref[0]
-        b_ref[0:128, :] = lat[128:256]
-        b_ref[128:PIECE, :] = rot_ref[1]
-
-    @pl.when(pl.program_id(0) == 1)
-    def _():
-        q_ref[...] = lat
-
-
-def down(rows, w, gains, rot):
-    piece = jax.ShapeDtypeStruct((PIECE, RANK), bf16)
+    return normed(lat, gain_ref[...]).astype(bf16)
+
+
+def kv_down_kernel(rows_ref, w_ref, gain_ref, rot_ref, a_ref, b_ref):
+    lat = latent(rows_ref, w_ref, gain_ref)
+    a_ref[0:128, :] = lat[0:128]
+    a_ref[128:PIECE, :] = rot_ref[0]
+    b_ref[0:128, :] = lat[128:256]
+    b_ref[128:PIECE, :] = rot_ref[1]
+
+
+def q_down_kernel(rows_ref, w_ref, gain_ref, q_ref):
+    q_ref[...] = latent(rows_ref, w_ref, gain_ref)
+
+
+def down(kernel, which, out, rows, w, gain, *rot):
+    def whole(shape):
+        return pl.BlockSpec(shape, lambda n: (0,) * len(shape))
+
     return pl.pallas_call(
-        down_kernel,
-        grid=(2,),
+        kernel,
+        grid=(1,),
         in_specs=[
-            pl.BlockSpec((ROWS, 2048), lambda n: (0, 0)),
-            pl.BlockSpec((16, 1, 128, RANK), lambda n: (0, n, 0, 0)),
-            pl.BlockSpec((1, 1, RANK), lambda n: (n, 0, 0)),
-            pl.BlockSpec((2, 16, RANK), lambda n: (0, 0, 0)),
-        ],
-        out_specs=(
-            pl.BlockSpec((PIECE, RANK), lambda n: (0, 0)),
-            pl.BlockSpec((PIECE, RANK), lambda n: (0, 0)),
-            pl.BlockSpec((ROWS, RANK), lambda n: (0, 0)),
-        ),
-        out_shape=(piece, piece, jax.ShapeDtypeStruct((ROWS, RANK), bf16)),
+            whole(rows.shape),
+            pl.BlockSpec((16, 1, 128, RANK), lambda n: (0, which, 0, 0)),
+            whole(gain.shape),
+        ]
+        + [whole(r.shape) for r in rot],
+        out_specs=tuple(whole(shape) for shape in out),
+        out_shape=tuple(jax.ShapeDtypeStruct(shape, bf16) for shape in out),
         compiler_params=limit(60, dimension_semantics=("arbitrary",)),
         name="down",
-    )(rows, w, gains, rot)
+    )(rows, w, gain, *rot)
 
 
 def reader(low, high=None):
@@ -407,8 +406,9 @@
     )
     w_full = lax.all_gather(w_out, "dp", axis=1, tiled=True)
 
-    gains = jnp.stack([kv_gain, q_gain]).reshape(2, 1, RANK)
-    a, b, qn = down(own, w_down, gains, packed)
+    gain = kv_gain.reshape(1, RANK)
+    a, b = down(kv_down_kernel, 0, ((PIECE, RANK),) * 2, own, w_down, gain, packed)
+    (qn,) = down(q_down_kernel, 1, ((ROWS, RANK),), own, w_down, q_gain.reshape(1, RANK))
 
     b1, b2, b3 = (lax.ppermute(b, "sp", x_shift(k)) for k in (1, 2, 3))
     a1, a2, a3 = (lax.ppermute(a, "sp", y_shift(k)) for k in (1, 2, 3))

time: 171 us -> 172 us (level)
  the two profiles are of different devices: /device:TPU:6 before, /device:TPU:32 now
where the time goes in v1:
time: 172 us; the launch traced here: 169 us
  waiting for transfers between devices  60.6 us (35%)
  starting transfers between devices  44.1 us (26%)
  Pallas kernels  35.8 us (21%)
  between operations  13.8 us (8%)
  local copies, waits for them, and re-layouts  10.3 us (6%)
  other arithmetic  2.73 us (2%)
    ppermute x3, waiting for transfers between devices, body(): a1, a2, a3 = (lax.ppermute(a, 'sp', y_shift(k)) for k in (1, 2, 3))  19.9 us
    pallas_call x1, Pallas kernels, attend(): pl.pallas_call(attend_kernel, grid=(LOCAL // PAIR, SIDE), in_specs=[SMEM]...  18.8 us
    all_gather x1, waiting for transfers between devices, body(): w_down = lax.all_gather(jnp.stack([w_kvdown, w_qdown]), 'dp')  10.7 us
    ppermute x3, waiting for transfers between devices, z_blocks(): ahead = lax.ppermute(ahead, 'dp', z_shift(1))  7.76 us
    ppermute x1, waiting for transfers between devices, z_blocks(): blocks[4] = lax.ppermute(ahead, 'dp', z_shift(1))  7.56 us
    unnamed x27, local copies, waits for them, and re-layouts  7.27 us
    ppermute x1, waiting for transfers between devices, body(): col1 = lax.ppermute(col, 'sp', x_shift(1))  6.98 us
    pallas_call x2, Pallas kernels, down(): pl.pallas_call(kernel, grid=(1,), in_specs=[whole(rows.shape), pl.BlockSp...  6.82 us
  transfers between devices with their start and end apart: 27, of which 11 were waited for; matrix products, arithmetic and copies ran while one was open for 6% of the time, Pallas kernels for 19%

profile of v1, /device:TPU:32, one launch (start us, length us, event | category | flops | bytes accessed | tf_op | source)
XLA Modules:
  0.0 169.0 jit_solution(2068707621230538060)
XLA Ops:
  12.8 3.2 %collective-permute-done = bf16[32,2048]{1,0:T(8,128)(2,1)S(1)} collective-permute-done((bf16[32,2048]{1,0:T(8,128)(2,1)S(1)}, bf16[32,2048]{1,0:T(8,128)(2,1)S(1)}, u32[]{:S(2)}, u32[]{:S(2)}) %collective-permute-start) | collective-permute-done | bytes 131104 | tf_op jit(solution)/shard_map/ppermute | solution.py:41
  17.9 2.3 %collective-permute-start.5 = (bf16[32,2048]{1,0:T(8,128)(2,1)S(1)}, bf16[32,2048]{1,0:T(8,128)(2,1)S(1)}, u32[]{:S(2)}, u32[]{:S(2)}) collective-permute-start(bf16[32,2048]{1,0:T(8,128)(2,1)S(1)} %collective-permute-done.4), channel_id=1, source_target_pairs={{0,14},{1,15},{2,0},{3,1},{4,2},{5,3},{6,4},{7,5},{8,6},{9,7},{10,... | collective-permute-start | bytes 393224 | tf_op jit(solution)/shard_map/ppermute | solution.py:42
  20.2 2.9 %collective-permute-done.1 = bf16[32,2048]{1,0:T(8,128)(2,1)S(1)} collective-permute-done((bf16[32,2048]{1,0:T(8,128)(2,1)S(1)}, bf16[32,2048]{1,0:T(8,128)(2,1)S(1)}, u32[]{:S(2)}, u32[]{:S(2)}) %collective-permute-start.1) | collective-permute-done | bytes 131104 | tf_op jit(solution)/shard_map/ppermute | solution.py:41
  23.9 4.4 %collective-permute-start.6 = (bf16[32,2048]{1,0:T(8,128)(2,1)S(1)}, bf16[32,2048]{1,0:T(8,128)(2,1)S(1)}, u32[]{:S(2)}, u32[]{:S(2)}) collective-permute-start(bf16[32,2048]{1,0:T(8,128)(2,1)S(1)} %collective-permute-done.5), channel_id=1, source_target_pairs={{0,14},{1,15},{2,0},{3,1},{4,2},{5,3},{6,4},{7,5},{8,6},{9,7},{10,... | collective-permute-start | bytes 393224 | tf_op jit(solution)/shard_map/ppermute | solution.py:42
  29.9 3.6 %collective-permute-start.3 = (bf16[32,2048]{1,0:T(8,128)(2,1)S(1)}, bf16[32,2048]{1,0:T(8,128)(2,1)S(1)}, u32[]{:S(2)}, u32[]{:S(2)}) collective-permute-start(bf16[32,2048]{1,0:T(8,128)(2,1)S(1)} %collective-permute-done.2), channel_id=1, source_target_pairs={{0,2},{1,3},{2,4},{3,5},{4,6},{5,7},{6,8},{7,9},{8,10},{9,11},{10,... | collective-permute-start | bytes 393224 | tf_op jit(solution)/shard_map/ppermute | solution.py:45
  33.5 7.6 %collective-permute-done.3 = bf16[32,2048]{1,0:T(8,128)(2,1)S(1)} collective-permute-done((bf16[32,2048]{1,0:T(8,128)(2,1)S(1)}, bf16[32,2048]{1,0:T(8,128)(2,1)S(1)}, u32[]{:S(2)}, u32[]{:S(2)}) %collective-permute-start.3) | collective-permute-done | bytes 131104 | tf_op jit(solution)/shard_map/ppermute | solution.py:45
  44.5 10.7 %all-gather.6.cloned.1.call-done = bf16[32,128,512]{2,1,0:T(8,128)(2,1)} async-done(((bf16[2,128,512]{2,1,0:T(8,128)(2,1)}), bf16[32,128,512]{2,1,0:T(8,128)(2,1)}) %all-gather.6.cloned.1.call-update) | async-done | bytes 4194320 | tf_op jit(solution)/shard_map/all_gather | solution.py:380
  55.2 3.4 %down.2 = (bf16[144,512]{1,0:T(8,128)(2,1)}, bf16[144,512]{1,0:T(8,128)(2,1)}) custom-call(bf16[256,2048]{1,0:T(8,128)(2,1)} %bitcast.36, bf16[16,2,128,512]{3,2,1,0:T(8,128)(2,1)} %bitcast.34, f32[1,512]{1,0:T(1,128)} %bitcast.46, bf16[2,16,512]{2,1,0:T(8,128)(2,1)} %reshape.93.rot_ref), custom_call_target="tpu_custom_call" | custom-call | tf_op jit(solution)/shard_map/down/pallas_call | solution.py:93
  60.1 2.7 %collective-permute-start.16 = (bf16[144,512]{1,0:T(8,128)(2,1)}, bf16[144,512]{1,0:T(8,128)(2,1)}, u32[]{:S(2)}, u32[]{:S(2)}) collective-permute-start(bf16[144,512]{1,0:T(8,128)(2,1)} %get-tuple-element.33), channel_id=1, source_target_pairs={{0,32},{16,48},{32,0},{48,16},{64,96},{80,112},{96,64},{112,80},{1... | collective-permute-start | bytes 442376 | tf_op jit(solution)/shard_map/ppermute | solution.py:413
  66.8 3.5 %collective-permute-start.9 = (bf16[144,512]{1,0:T(8,128)(2,1)}, bf16[144,512]{1,0:T(8,128)(2,1)S(1)}, u32[]{:S(2)}, u32[]{:S(2)}) collective-permute-start(bf16[144,512]{1,0:T(8,128)(2,1)} %get-tuple-element.32), channel_id=1, source_target_pairs={{0,128},{16,144},{32,160},{48,176},{64,192},{80,208},{96,224},{112... | collective-permute-start | bytes 442376 | tf_op jit(solution)/shard_map/ppermute | solution.py:414
  70.4 3.4 %down.3 = bf16[256,512]{1,0:T(8,128)(2,1)} custom-call(bf16[256,2048]{1,0:T(8,128)(2,1)} %bitcast.37, bf16[16,2,128,512]{3,2,1,0:T(8,128)(2,1)} %bitcast.35, f32[1,512]{1,0:T(1,128)} %bitcast.45), custom_call_target="tpu_custom_call" | custom-call | tf_op jit(solution)/shard_map/down/pallas_call | solution.py:93
  77.7 3.2 %collective-permute-start.20 = (bf16[832,512]{1,0:T(8,128)(2,1)S(1)}, bf16[832,512]{1,0:T(8,128)(2,1)S(1)}, u32[]{:S(2)}, u32[]{:S(2)}) collective-permute-start(bf16[832,512]{1,0:T(8,128)(2,1)S(1)} %constant_dynamic-update-slice_fusion.21.b0), channel_id=1, source_target_pairs={{0,192},{16,208},{32,224},{48,240},{64,0},{80,16},{96,32},{112,48}... | collective-permute-start | bytes 2555912 | tf_op jit(solution)/shard_map/ppermute | solution.py:420
  81.1 19.9 %collective-permute-done.10 = bf16[144,512]{1,0:T(8,128)(2,1)S(1)} collective-permute-done((bf16[144,512]{1,0:T(8,128)(2,1)S(1)}, bf16[144,512]{1,0:T(8,128)(2,1)S(1)}, u32[]{:S(2)}, u32[]{:S(2)}) %collective-permute-start.10) | collective-permute-done | bytes 147488 | tf_op jit(solution)/shard_map/ppermute | solution.py:414
  101.6 2.7 %collective-permute-start.13 = (bf16[576,512]{1,0:T(8,128)(2,1)S(1)}, bf16[576,512]{1,0:T(8,128)(2,1)S(1)}, u32[]{:S(2)}, u32[]{:S(2)}) collective-permute-start(bf16[576,512]{1,0:T(8,128)(2,1)S(1)} %constant_dynamic-update-slice_fusion.17.a0), channel_id=1, source_target_pairs={{0,48},{16,0},{32,16},{48,32},{64,112},{80,64},{96,80},{112,96},{1... | collective-permute-start | bytes 1769480 | tf_op jit(solution)/shard_map/ppermute | solution.py:418
  104.5 3.8 %collective-permute-start.21 = (bf16[416,512]{1,0:T(8,128)(2,1)S(1)}, bf16[416,512]{1,0:T(8,128)(2,1)S(1)}, u32[]{:S(2)}, u32[]{:S(2)}) collective-permute-start(bf16[416,512]{1,0:T(8,128)(2,1)S(1)} %slice.65), channel_id=1, source_target_pairs={{0,192},{16,208},{32,224},{48,240},{64,0},{80,16},{96,32},{112,48}... | collective-permute-start | bytes 1277960 | tf_op jit(solution)/shard_map/ppermute | solution.py:424
  108.3 7.0 %collective-permute-done.11.a1 = bf16[576,512]{1,0:T(8,128)(2,1)S(1)} collective-permute-done((bf16[576,512]{1,0:T(8,128)(2,1)S(1)}, bf16[576,512]{1,0:T(8,128)(2,1)S(1)}, u32[]{:S(2)}, u32[]{:S(2)}) %collective-permute-start.11) | collective-permute-done | bytes 589856 | tf_op jit(solution)/shard_map/ppermute | solution.py:417
  115.4 3.5 %collective-permute-start.14 = (bf16[288,512]{1,0:T(8,128)(2,1)S(1)}, bf16[288,512]{1,0:T(8,128)(2,1)S(1)}, u32[]{:S(2)}, u32[]{:S(2)}) collective-permute-start(bf16[288,512]{1,0:T(8,128)(2,1)S(1)} %slice.63), channel_id=1, source_target_pairs={{0,48},{16,0},{32,16},{48,32},{64,112},{80,64},{96,80},{112,96},{1... | collective-permute-start | bytes 884744 | tf_op jit(solution)/shard_map/ppermute | solution.py:422
  118.9 5.8 %early.1 = (bf16[2,4096,256]{2,1,0:T(8,128)(2,1)S(1)}, bf16[4096,128]{1,0:T(8,128)(2,1)S(1)}, bf16[2,256,4096]{2,1,0:T(8,128)(2,1)S(1)}, bf16[4,1024,256]{2,1,0:...) custom-call(s32[4]{0:T(128)S(1)} %pad_add_fusion.yx_ref, ...), custom_call_target="tpu_custom_call" | custom-call | tf_op jit(solution)/shard_map/early/pallas_call | solution.py:187
  124.8 18.8 %attend.1 = (bf16[512,256]{1,0:T(8,128)(2,1)S(1)}, bf16[512,256]{1,0:T(8,128)(2,1)S(1)}, bf16[512,256]{1,0:T(8,128)(2,1)S(1)}, bf16[512,256]{1,0:T(8,128)(2,1)S(1)}) custom-call(s32[4]{0:T(128)S(1)} %pad_add_fusion.yx_ref, bf16[288,512]{1,0:T(8,128)(2,1)S(1)} %collective-permute-done.12.a2l, bf16[288,512]{1,0:T(8,128)(2,1)S(1)} %collective-permute-done.14.a2h, ...), custom_call_target="tpu_custom_call" | custom-call | tf_op jit(solution)/shard_map/attend/pallas_call | solution.py:296
  143.6 3.7 %collective-permute-start.22 = (bf16[512,256]{1,0:T(8,128)(2,1)S(1)}, bf16[512,256]{1,0:T(8,128)(2,1)S(1)}, u32[]{:S(2)}, u32[]{:S(2)}) collective-permute-start(bf16[512,256]{1,0:T(8,128)(2,1)S(1)} %get-tuple-element.49), channel_id=1, source_target_pairs={{0,192},{16,208},{32,224},{48,240},{64,0},{80,16},{96,32},{112,48}... | collective-permute-start | bytes 786440 | tf_op jit(solution)/shard_map/ppermute | solution.py:432
  148.3 3.4 %copy-done.1 = bf16[2048,2048]{1,0:T(8,128)(2,1)S(1)} copy-done((bf16[2048,2048]{1,0:T(8,128)(2,1)S(1)}, bf16[2048,2048]{1,0:T(8,128)(2,1)}, u32[]{:S(2)}) %copy-start.1) | copy-done | bytes 8388632
  152.2 2.7 %collective-permute-done.22.p1 = bf16[512,256]{1,0:T(8,128)(2,1)S(1)} collective-permute-done((bf16[512,256]{1,0:T(8,128)(2,1)S(1)}, bf16[512,256]{1,0:T(8,128)(2,1)S(1)}, u32[]{:S(2)}, u32[]{:S(2)}) %collective-permute-start.22) | collective-permute-done | bytes 262176 | tf_op jit(solution)/shard_map/ppermute | solution.py:432
  156.0 2.4 %collective-permute-done.24.p3 = bf16[512,256]{1,0:T(8,128)(2,1)S(1)} collective-permute-done((bf16[512,256]{1,0:T(8,128)(2,1)S(1)}, bf16[512,256]{1,0:T(8,128)(2,1)S(1)}, u32[]{:S(2)}, u32[]{:S(2)}) %collective-permute-start.24) | collective-permute-done | bytes 262176 | tf_op jit(solution)/shard_map/ppermute | solution.py:432
  158.4 3.8 %project.1 = bf16[256,2048]{1,0:T(8,128)(2,1)} custom-call(s32[1]{0:T(128)} %bitcast.y_ref, bf16[512,256]{1,0:T(8,128)(2,1)S(1)} %get-tuple-element.48.p0, bf16[512,256]{1,0:T(8,128)(2,1)S(1)} %collective-permute-done.22.p1, bf16[512,256]{1,0:T(8,128)(2,1)S(1)} %collective-permute-done.23.p2, bf16[512,256]{1,0:T(8,128)(2,1)S(1)} %collective-permute-done.24.p3, ...), custom_call_target="tpu_custom_call" | custom-call | tf_op jit(solution)/shard_map/project/pallas_call | solution.py:330
  (94 shorter events, 26.7 us)
Async XLA Ops:
  6.5 48.6 %all-gather.6.cloned.1.call-start = ((), (), s32[]{:S(2)}) async-start(), calls=%async_computation.1 | async-start | bytes 4456448 | tf_op jit(solution)/shard_map/all_gather | solution.py:380
  8.3 135.2 %all-gather.4.cloned.1.call-start = ((), (), s32[]{:S(2)}) async-start(), calls=%async_computation | async-start | bytes 8912896 | tf_op jit(solution)/shard_map/all_gather | solution.py:407
  16.0 7.2 %collective-permute-start.1 = (bf16[32,2048]{1,0:T(8,128)(2,1)S(1)}, bf16[32,2048]{1,0:T(8,128)(2,1)S(1)}, u32[]{:S(2)}, u32[]{:S(2)}) collective-permute-start(bf16[32,2048]{1,0:T(8,128)(2,1)S(1)} %collective-permute-done), channel_id=1, source_target_pairs={{0,2},{1,3},{2,4},{3,5},{4,6},{5,7},{6,8},{7,9},{8,10},{9,11},{10,... | collective-permute-start | bytes 393224 | tf_op jit(solution)/shard_map/ppermute | solution.py:41
  17.9 6.0 %collective-permute-start.5 = (bf16[32,2048]{1,0:T(8,128)(2,1)S(1)}, bf16[32,2048]{1,0:T(8,128)(2,1)S(1)}, u32[]{:S(2)}, u32[]{:S(2)}) collective-permute-start(bf16[32,2048]{1,0:T(8,128)(2,1)S(1)} %collective-permute-done.4), channel_id=1, source_target_pairs={{0,14},{1,15},{2,0},{3,1},{4,2},{5,3},{6,4},{7,5},{8,6},{9,7},{10,... | collective-permute-start | bytes 393224 | tf_op jit(solution)/shard_map/ppermute | solution.py:42
  23.1 6.8 %collective-permute-start.2 = (bf16[32,2048]{1,0:T(8,128)(2,1)S(1)}, bf16[32,2048]{1,0:T(8,128)(2,1)S(1)}, u32[]{:S(2)}, u32[]{:S(2)}) collective-permute-start(bf16[32,2048]{1,0:T(8,128)(2,1)S(1)} %collective-permute-done.1), channel_id=1, source_target_pairs={{0,2},{1,3},{2,4},{3,5},{4,6},{5,7},{6,8},{7,9},{8,10},{9,11},{10,... | collective-permute-start | bytes 393224 | tf_op jit(solution)/shard_map/ppermute | solution.py:41
  23.9 17.2 %collective-permute-start.6 = (bf16[32,2048]{1,0:T(8,128)(2,1)S(1)}, bf16[32,2048]{1,0:T(8,128)(2,1)S(1)}, u32[]{:S(2)}, u32[]{:S(2)}) collective-permute-start(bf16[32,2048]{1,0:T(8,128)(2,1)S(1)} %collective-permute-done.5), channel_id=1, source_target_pairs={{0,14},{1,15},{2,0},{3,1},{4,2},{5,3},{6,4},{7,5},{8,6},{9,7},{10,... | collective-permute-start | bytes 393224 | tf_op jit(solution)/shard_map/ppermute | solution.py:42
  29.9 11.1 %collective-permute-start.3 = (bf16[32,2048]{1,0:T(8,128)(2,1)S(1)}, bf16[32,2048]{1,0:T(8,128)(2,1)S(1)}, u32[]{:S(2)}, u32[]{:S(2)}) collective-permute-start(bf16[32,2048]{1,0:T(8,128)(2,1)S(1)} %collective-permute-done.2), channel_id=1, source_target_pairs={{0,2},{1,3},{2,4},{3,5},{4,6},{5,7},{6,8},{7,9},{8,10},{9,11},{10,... | collective-permute-start | bytes 393224 | tf_op jit(solution)/shard_map/ppermute | solution.py:45
  58.6 15.2 %collective-permute-start.15 = (bf16[144,512]{1,0:T(8,128)(2,1)}, bf16[144,512]{1,0:T(8,128)(2,1)}, u32[]{:S(2)}, u32[]{:S(2)}) collective-permute-start(bf16[144,512]{1,0:T(8,128)(2,1)} %get-tuple-element.33), channel_id=1, source_target_pairs={{0,16},{16,32},{32,48},{48,0},{64,80},{80,96},{96,112},{112,64},{1... | collective-permute-start | bytes 442376 | tf_op jit(solution)/shard_map/ppermute | solution.py:413
  60.1 14.6 %collective-permute-start.16 = (bf16[144,512]{1,0:T(8,128)(2,1)}, bf16[144,512]{1,0:T(8,128)(2,1)}, u32[]{:S(2)}, u32[]{:S(2)}) collective-permute-start(bf16[144,512]{1,0:T(8,128)(2,1)} %get-tuple-element.33), channel_id=1, source_target_pairs={{0,32},{16,48},{32,0},{48,16},{64,96},{80,112},{96,64},{112,80},{1... | collective-permute-start | bytes 442376 | tf_op jit(solution)/shard_map/ppermute | solution.py:413
  63.7 11.9 %collective-permute-start.17 = (bf16[144,512]{1,0:T(8,128)(2,1)}, bf16[144,512]{1,0:T(8,128)(2,1)}, u32[]{:S(2)}, u32[]{:S(2)}) collective-permute-start(bf16[144,512]{1,0:T(8,128)(2,1)} %get-tuple-element.33), channel_id=1, source_target_pairs={{0,48},{16,0},{32,16},{48,32},{64,112},{80,64},{96,80},{112,96},{1... | collective-permute-start | bytes 442376 | tf_op jit(solution)/shard_map/ppermute | solution.py:413
  65.5 15.6 %collective-permute-start.8 = (bf16[144,512]{1,0:T(8,128)(2,1)}, bf16[144,512]{1,0:T(8,128)(2,1)S(1)}, u32[]{:S(2)}, u32[]{:S(2)}) collective-permute-start(bf16[144,512]{1,0:T(8,128)(2,1)} %get-tuple-element.32), channel_id=1, source_target_pairs={{0,64},{16,80},{32,96},{48,112},{64,128},{80,144},{96,160},{112,17... | collective-permute-start | bytes 442376 | tf_op jit(solution)/shard_map/ppermute | solution.py:414
  66.8 14.2 %collective-permute-start.9 = (bf16[144,512]{1,0:T(8,128)(2,1)}, bf16[144,512]{1,0:T(8,128)(2,1)S(1)}, u32[]{:S(2)}, u32[]{:S(2)}) collective-permute-start(bf16[144,512]{1,0:T(8,128)(2,1)} %get-tuple-element.32), channel_id=1, source_target_pairs={{0,128},{16,144},{32,160},{48,176},{64,192},{80,208},{96,224},{112... | collective-permute-start | bytes 442376 | tf_op jit(solution)/shard_map/ppermute | solution.py:414
  77.6 26.8 %collective-permute-start.18 = (bf16[832,512]{1,0:T(8,128)(2,1)S(1)}, bf16[832,512]{1,0:T(8,128)(2,1)S(1)}, u32[]{:S(2)}, u32[]{:S(2)}) collective-permute-start(bf16[832,512]{1,0:T(8,128)(2,1)S(1)} %constant_dynamic-update-slice_fusion.21.b0), channel_id=1, source_target_pairs={{0,64},{16,80},{32,96},{48,112},{64,128},{80,144},{96,160},{112,17... | collective-permute-start | bytes 2555912 | tf_op jit(solution)/shard_map/ppermute | solution.py:419
  77.7 26.8 %collective-permute-start.20 = (bf16[832,512]{1,0:T(8,128)(2,1)S(1)}, bf16[832,512]{1,0:T(8,128)(2,1)S(1)}, u32[]{:S(2)}, u32[]{:S(2)}) collective-permute-start(bf16[832,512]{1,0:T(8,128)(2,1)S(1)} %constant_dynamic-update-slice_fusion.21.b0), channel_id=1, source_target_pairs={{0,192},{16,208},{32,224},{48,240},{64,0},{80,16},{96,32},{112,48}... | collective-permute-start | bytes 2555912 | tf_op jit(solution)/shard_map/ppermute | solution.py:420
  80.9 20.1 %collective-permute-start.10 = (bf16[144,512]{1,0:T(8,128)(2,1)S(1)}, bf16[144,512]{1,0:T(8,128)(2,1)S(1)}, u32[]{:S(2)}, u32[]{:S(2)}) collective-permute-start(bf16[144,512]{1,0:T(8,128)(2,1)S(1)} %copy-done.4), channel_id=1, source_target_pairs={{0,192},{16,208},{32,224},{48,240},{64,0},{80,16},{96,32},{112,48}... | collective-permute-start | bytes 442376 | tf_op jit(solution)/shard_map/ppermute | solution.py:414
  101.0 14.2 %collective-permute-start.11 = (bf16[576,512]{1,0:T(8,128)(2,1)S(1)}, bf16[576,512]{1,0:T(8,128)(2,1)S(1)}, u32[]{:S(2)}, u32[]{:S(2)}) collective-permute-start(bf16[576,512]{1,0:T(8,128)(2,1)S(1)} %constant_dynamic-update-slice_fusion.17.a0), channel_id=1, source_target_pairs={{0,16},{16,32},{32,48},{48,0},{64,80},{80,96},{96,112},{112,64},{1... | collective-permute-start | bytes 1769480 | tf_op jit(solution)/shard_map/ppermute | solution.py:417
  101.6 13.8 %collective-permute-start.13 = (bf16[576,512]{1,0:T(8,128)(2,1)S(1)}, bf16[576,512]{1,0:T(8,128)(2,1)S(1)}, u32[]{:S(2)}, u32[]{:S(2)}) collective-permute-start(bf16[576,512]{1,0:T(8,128)(2,1)S(1)} %constant_dynamic-update-slice_fusion.17.a0), channel_id=1, source_target_pairs={{0,48},{16,0},{32,16},{48,32},{64,112},{80,64},{96,80},{112,96},{1... | collective-permute-start | bytes 1769480 | tf_op jit(solution)/shard_map/ppermute | solution.py:418
  104.4 20.4 %collective-permute-start.19 = (bf16[416,512]{1,0:T(8,128)(2,1)S(1)}, bf16[416,512]{1,0:T(8,128)(2,1)S(1)}, u32[]{:S(2)}, u32[]{:S(2)}) collective-permute-start(bf16[416,512]{1,0:T(8,128)(2,1)S(1)} %slice.64), channel_id=1, source_target_pairs={{0,64},{16,80},{32,96},{48,112},{64,128},{80,144},{96,160},{112,17... | collective-permute-start | bytes 1277960 | tf_op jit(solution)/shard_map/ppermute | solution.py:423
  104.5 20.3 %collective-permute-start.21 = (bf16[416,512]{1,0:T(8,128)(2,1)S(1)}, bf16[416,512]{1,0:T(8,128)(2,1)S(1)}, u32[]{:S(2)}, u32[]{:S(2)}) collective-permute-start(bf16[416,512]{1,0:T(8,128)(2,1)S(1)} %slice.65), channel_id=1, source_target_pairs={{0,192},{16,208},{32,224},{48,240},{64,0},{80,16},{96,32},{112,48}... | collective-permute-start | bytes 1277960 | tf_op jit(solution)/shard_map/ppermute | solution.py:424
  115.3 9.4 %collective-permute-start.12 = (bf16[288,512]{1,0:T(8,128)(2,1)S(1)}, bf16[288,512]{1,0:T(8,128)(2,1)S(1)}, u32[]{:S(2)}, u32[]{:S(2)}) collective-permute-start(bf16[288,512]{1,0:T(8,128)(2,1)S(1)} %slice.62), channel_id=1, source_target_pairs={{0,16},{16,32},{32,48},{48,0},{64,80},{80,96},{96,112},{112,64},{1... | collective-permute-start | bytes 884744 | tf_op jit(solution)/shard_map/ppermute | solution.py:421
  115.4 9.3 %collective-permute-start.14 = (bf16[288,512]{1,0:T(8,128)(2,1)S(1)}, bf16[288,512]{1,0:T(8,128)(2,1)S(1)}, u32[]{:S(2)}, u32[]{:S(2)}) collective-permute-start(bf16[288,512]{1,0:T(8,128)(2,1)S(1)} %slice.63), channel_id=1, source_target_pairs={{0,48},{16,0},{32,16},{48,32},{64,112},{80,64},{96,80},{112,96},{1... | collective-permute-start | bytes 884744 | tf_op jit(solution)/shard_map/ppermute | solution.py:422
  143.6 11.4 %collective-permute-start.22 = (bf16[512,256]{1,0:T(8,128)(2,1)S(1)}, bf16[512,256]{1,0:T(8,128)(2,1)S(1)}, u32[]{:S(2)}, u32[]{:S(2)}) collective-permute-start(bf16[512,256]{1,0:T(8,128)(2,1)S(1)} %get-tuple-element.49), channel_id=1, source_target_pairs={{0,192},{16,208},{32,224},{48,240},{64,0},{80,16},{96,32},{112,48}... | collective-permute-start | bytes 786440 | tf_op jit(solution)/shard_map/ppermute | solution.py:432
  147.3 8.7 %collective-permute-start.23 = (bf16[512,256]{1,0:T(8,128)(2,1)S(1)}, bf16[512,256]{1,0:T(8,128)(2,1)S(1)}, u32[]{:S(2)}, u32[]{:S(2)}) collective-permute-start(bf16[512,256]{1,0:T(8,128)(2,1)S(1)} %get-tuple-element.50), channel_id=1, source_target_pairs={{0,128},{16,144},{32,160},{48,176},{64,192},{80,208},{96,224},{112... | collective-permute-start | bytes 786440 | tf_op jit(solution)/shard_map/ppermute | solution.py:432
  147.3 11.1 %collective-permute-start.24 = (bf16[512,256]{1,0:T(8,128)(2,1)S(1)}, bf16[512,256]{1,0:T(8,128)(2,1)S(1)}, u32[]{:S(2)}, u32[]{:S(2)}) collective-permute-start(bf16[512,256]{1,0:T(8,128)(2,1)S(1)} %get-tuple-element.51), channel_id=1, source_target_pairs={{0,64},{16,80},{32,96},{48,112},{64,128},{80,144},{96,160},{112,17... | collective-permute-start | bytes 786440 | tf_op jit(solution)/shard_map/ppermute | solution.py:432
  (8 other events, 85.0 us)
Sparse Core Ops, SparseCore 0:
  9.2 45.9 all-gather.5
  56.9 64.0 all-gather.3
